TPU v7x, 512 devices: a whole 4x8x8 slice. The times are simulated.
512 devices in a mesh: fs: 64 (over z, y), tp: 8 (over x, core).
Axes of the slice: x: 4, y: 8, z: 8, core: 2. Of those that a mesh axis runs over, the one named last changes fastest.
Arguments:
- tokens: bfloat16 [24576, 2048], P('fs', 'tp'), may hold values from -6 to 6
- outer_gate: bfloat16 [2048, 2048], P('fs', 'tp'), may hold values from -0.125 to 0.125
- inner_gate: bfloat16 [2048, 2048], P('fs', 'tp'), may hold values from -0.125 to 0.125
- mix_value: bfloat16 [2048, 2048], P('fs', 'tp'), may hold values from -0.125 to 0.125
- mix_taps: bfloat16 [3, 2048], P(None, 'tp'), may hold values from -3 to 3
- mix_out: bfloat16 [2048, 2048], P('tp', 'fs'), may hold values from -0.375 to 0.375
- mix_gain: bfloat16 [2048], P('tp'), may hold values from 0.099609375 to 1.8984375
- ffn_gate: bfloat16 [2048, 3072], P('fs', 'tp'), may hold values from -0.125 to 0.125
- ffn_value: bfloat16 [2048, 3072], P('fs', 'tp'), may hold values from -0.125 to 0.125
- gate_taps: bfloat16 [3, 3072], P(None, 'tp'), may hold values from -3 to 3
- value_taps: bfloat16 [3, 3072], P(None, 'tp'), may hold values from -3 to 3
- ffn_down: bfloat16 [3072, 2048], P('tp', 'fs'), may hold values from -0.3125 to 0.3125
- ffn_gain: bfloat16 [2048], P('tp'), may hold values from 0.099609375 to 1.8984375
Outputs:
- layer_out: bfloat16 [24576, 2048], P('fs', 'tp')
All inputs are finite; a program needn't handle non-finite values.
Results may differ from a plain program's by a relative error of at most 0.015.
Values may be sent and summed in bfloat16 or wider, within the bound.
A program may use at most 64 MiB of HBM per device.

v0:
```python
import jax
import jax.numpy as jnp
from jax import lax
from jax.sharding import PartitionSpec as P

SEQ_LEN = 128
residual_scale = 8.0**0.25
norm_epsilon = 1e-05


def copy_for_each(value, axis):
    copies = jnp.broadcast_to(value, (lax.axis_size(axis), *value.shape))
    return lax.all_to_all(copies, axis, split_axis=0, concat_axis=0, tiled=True)


def taken_together(value, axis):
    everything = copy_for_each(value, axis)
    return jnp.sum(everything, axis=0)


def in_one(arrays, axis):
    ends = [0]
    for a in arrays:
        ends.append(ends[-1] + a.size)
    subtotal = taken_together(jnp.concatenate([a.ravel() for a in arrays]), axis)
    return tuple((subtotal[b:e].reshape(a.shape) for a, b, e in zip(arrays, ends, ends[1:])))


def in_one_piece(arrays, axis, dim, along):
    both = jnp.concatenate(arrays, axis=along)
    filled, at, finished = (lax.all_gather(both, axis, axis=dim, tiled=True), 0, [])
    for a in arrays:
        finished.append(lax.slice_in_dim(filled, at, at + a.shape[along], axis=along))
        at += a.shape[along]
    return tuple(finished)


def laid_out(blocks, dim):
    blocks = jnp.moveaxis(blocks, 0, dim)
    dims = blocks.shape
    return blocks.reshape(*dims[:dim], dims[dim] * dims[dim + 1], *dims[dim + 2 :])


def collect(value, axis, dim):
    return laid_out(copy_for_each(value, axis), dim)


def split_up(value, dim, peers):
    before, after = (value.shape[:dim], value.shape[dim + 1 :])
    return jnp.moveaxis(value.reshape(*before, peers, -1, *after), dim, 0)


def sent_and_summed(value, axis, dim):
    peers = lax.axis_size(axis)
    blocks = lax.all_to_all(split_up(value, dim, peers), axis, 0, 0, tiled=True)
    return jnp.sum(blocks.astype(jnp.float32), axis=0)


def stored(values):
    return lax.optimization_barrier(values.astype(jnp.bfloat16)).astype(jnp.float32)


def shift_rows(values, offset):
    position = jnp.arange(values.shape[0]) % SEQ_LEN
    shifted = jnp.concatenate(
        [jnp.zeros((offset, values.shape[1]), values.dtype), values[:-offset]], axis=0
    )
    return jnp.where((position >= offset)[:, None], shifted, jnp.zeros_like(shifted))


def causal_taps(values, taps):
    weights = taps.astype(jnp.float32)
    return (
        values * weights[2]
        + shift_rows(values, 1) * weights[1]
        + shift_rows(values, 2) * weights[0]
    )


def fold_rows(whole, pieces):
    return tuple((jnp.dot(whole, piece, preferred_element_type=jnp.float32) for piece in pieces))


def norm_shares(prenorm, gain):
    width = prenorm.shape[1] * lax.axis_size("tp")
    row_sums = jnp.sum(prenorm, axis=1)
    row_squares = jnp.sum(prenorm * prenorm, axis=1)
    total, total_squares = in_one((row_sums, row_squares), "tp")
    mean = total / width
    spread = total_squares / width - mean * mean
    scaled = (prenorm - mean[:, None]) * lax.rsqrt(spread[:, None] + norm_epsilon)
    return (scaled * gain.astype(jnp.float32)).astype(jnp.bfloat16)


def body(
    tokens,
    outer_gate,
    inner_gate,
    mix_value,
    mix_taps,
    mix_out,
    mix_gain,
    ffn_gate,
    ffn_value,
    gate_taps,
    value_taps,
    ffn_down,
    ffn_gain,
):
    gate_whole, value_whole = in_one_piece((ffn_gate, ffn_value), "fs", 0, 1)
    whole_tokens = collect(tokens, "tp", 1)
    outer, inner, values = fold_rows(
        whole_tokens, in_one_piece((outer_gate, inner_gate, mix_value), "fs", 0, 1)
    )
    outer, inner, values = (stored(outer), stored(inner), stored(values))
    gated = (outer * causal_taps(inner * values, mix_taps)).astype(jnp.bfloat16)
    mixer_terms = jnp.dot(gated, collect(mix_out, "fs", 1), preferred_element_type=jnp.float32)
    mixer_branch = sent_and_summed(mixer_terms.astype(jnp.bfloat16), "tp", 1)
    first_own = norm_shares(residual_scale * tokens.astype(jnp.float32) + mixer_branch, mix_gain)
    first_whole = collect(first_own, "tp", 1)
    gate_up = jnp.dot(first_whole, gate_whole, preferred_element_type=jnp.float32)
    value_up = jnp.dot(first_whole, value_whole, preferred_element_type=jnp.float32)
    gate_up, value_up = (stored(gate_up), stored(value_up))
    hidden = (
        jax.nn.silu(causal_taps(gate_up, gate_taps)) * causal_taps(value_up, value_taps)
    ).astype(jnp.bfloat16)
    ffn_terms = jnp.dot(
        hidden,
        lax.all_gather(ffn_down, "fs", axis=1, tiled=True),
        preferred_element_type=jnp.float32,
    )
    ffn_branch = sent_and_summed(ffn_terms.astype(jnp.bfloat16), "tp", 1)
    return norm_shares(residual_scale * first_own.astype(jnp.float32) + ffn_branch, ffn_gain)


def solution(mesh):
    placed = (
        P("fs", "tp"),
        P("fs", "tp"),
        P("fs", "tp"),
        P("fs", "tp"),
        P(None, "tp"),
        P("tp", "fs"),
        P("tp"),
        P("fs", "tp"),
        P("fs", "tp"),
        P(None, "tp"),
        P(None, "tp"),
        P("tp", "fs"),
        P("tp"),
    )
    return jax.shard_map(body, mesh=mesh, in_specs=placed, out_specs=P("fs", "tp"), check_vma=False)
```

profile of v0, /device:TPU:1, one launch (start us, length us, event | category | flops | bytes accessed | tf_op | source)
XLA Modules:
  0.0 324.7 jit_solution(7652189762097484057)
XLA Ops:
  6.5 0.0 all-gather.4.cloned.1.call-start
  6.5 1.4 pad_maximum_fusion
  7.9 0.0 all-gather.4.cloned.1.call-update
  7.9 0.0 all-gather.6.cloned.1.call-start
  8.0 1.4 pad_maximum_fusion.1
  9.4 0.0 all-gather.6.cloned.1.call-update
  9.4 1.1 copy.25
  10.5 0.1 broadcast_in_dim.65
  10.6 0.0 copy-start.1
  10.6 29.8 %all_to_all.37 = bf16[8,384,256]{1,2,0:T(8,128)(2,1)S(1)} all-to-all(bf16[8,384,256]{1,2,0:T(8,128)(2,1)S(1)} %broadcast_in_dim.65), channel_id=1, replica_groups=mesh['fs'=64,'tp'=8] {'tp'}, dimensions={0} | all-to-all | bytes 3145728 | tf_op jit(solution)/shard_map/all_to_all | solution.py:13
  40.5 0.0 copy-done.1
  40.5 1.1 broadcast_in_dim.68
  41.6 12.7 %all-to-all-start.1 = ((bf16[64,256,32]{1,2,0:T(8,128)(2,1)}), bf16[64,256,32]{1,2,0:T(8,128)(2,1)S(1)}, u32[]{:S(2)}, u32[]{:S(2)}) async-start(bf16[64,256,32]{1,2,0:T(8,128)(2,1)} %broadcast_in_dim.68), calls=%async_computation.1 | async-start | bytes 2097152 | tf_op jit(solution)/shard_map/all_to_all | solution.py:13
  54.3 0.0 copy-done.2
  54.3 0.0 copy-start.7
  54.3 0.0 copy-start.9
  54.3 53.7 %all-gather.4.cloned.1.call-done = bf16[2048,768]{1,0:T(8,128)(2,1)} async-done(((bf16[32,768]{1,0:T(8,128)(2,1)}), bf16[2048,768]{1,0:T(8,128)(2,1)}) %all-gather.4.cloned.1.call-update) | async-done | bytes 3145744 | tf_op jit(solution)/shard_map/all_gather | solution.py:31
  108.0 2.0 fusion.11
  110.0 2.0 fusion.12
  112.0 2.0 fusion.10
  114.0 0.0 all-to-all-done.1
  114.0 0.0 copy-done.7
  114.0 0.0 copy-done.9
  114.0 1.0 convolution_convert_fusion.1
  115.1 1.3 copy.42
  116.3 8.6 %all-to-all-start.2 = ((bf16[8,384,256]{2,1,0:T(8,128)(2,1)}), bf16[8,384,256]{2,1,0:T(8,128)(2,1)S(1)}, u32[]{:S(2)}, u32[]{:S(2)}) async-start(bf16[8,384,256]{2,1,0:T(8,128)(2,1)} %bitcast.38), calls=%async_computation.2 | async-start | bytes 3145728 | tf_op jit(solution)/shard_map/all_to_all | solution.py:55
  124.9 0.0 all-gather.8.cloned.1.call-start
  125.0 0.7 all-gather.8.cloned.1.call-update
  125.7 19.8 %all-to-all-done.2 = bf16[8,384,256]{2,1,0:T(8,128)(2,1)S(1)} async-done(((bf16[8,384,256]{2,1,0:T(8,128)(2,1)}), bf16[8,384,256]{2,1,0:T(8,128)(2,1)S(1)}, u32[]{:S(2)}, u32[]{:S(2)}) %all-to-all-start.2) | async-done | bytes 1572896 | tf_op jit(solution)/shard_map/all_to_all | solution.py:55
  145.5 0.2 convert_reduce_fusion.1
  145.7 0.0 copy-done
  145.7 0.2 fusion.34
  145.9 0.6 broadcast_in_dim.69
  146.6 4.2 %all-to-all-start.3 = ((f32[8,1,768]{2,1,0:T(1,128)}), f32[8,1,768]{2,1,0:T(1,128)S(1)}, u32[]{:S(2)}, u32[]{:S(2)}) async-start(f32[8,1,768]{2,1,0:T(1,128)} %broadcast_in_dim.69), calls=%async_computation.3 | async-start | bytes 49152 | tf_op jit(solution)/shard_map/all_to_all | solution.py:13
  150.8 0.0 copy-done.12
  150.8 4.7 %all-to-all-done.3 = f32[8,1,768]{2,1,0:T(1,128)S(1)} async-done(((f32[8,1,768]{2,1,0:T(1,128)}), f32[8,1,768]{2,1,0:T(1,128)S(1)}, u32[]{:S(2)}, u32[]{:S(2)}) %all-to-all-start.3) | async-done | bytes 24608 | tf_op jit(solution)/shard_map/all_to_all | solution.py:13
  155.5 0.2 multiply_convert_fusion.2
  155.7 0.2 copy.28
  155.9 1.3 broadcast_in_dim.70
  157.2 4.3 %all-to-all-start.4 = ((bf16[8,384,256]{1,2,0:T(8,128)(2,1)}), bf16[8,384,256]{1,2,0:T(8,128)(2,1)S(1)}, u32[]{:S(2)}, u32[]{:S(2)}) async-start(bf16[8,384,256]{1,2,0:T(8,128)(2,1)} %broadcast_in_dim.70), calls=%async_computation.4 | async-start | bytes 3145728 | tf_op jit(solution)/shard_map/all_to_all | solution.py:13
  161.5 0.0 copy-done.3
  161.5 0.0 copy-done.4
  161.5 0.6 slice_reduce_fusion.2
  162.2 30.5 %all-gather.6.cloned.1.call-done = bf16[2048,768]{1,0:T(8,128)(2,1)} async-done(((bf16[32,768]{1,0:T(8,128)(2,1)}), bf16[2048,768]{1,0:T(8,128)(2,1)}) %all-gather.6.cloned.1.call-update) | async-done | bytes 3145744 | tf_op jit(solution)/shard_map/all_gather | solution.py:31
  192.7 0.0 all-to-all-done.4
  192.7 2.6 fusion.4
  195.3 0.0 copy-done.11
  195.4 1.0 fusion.7
  196.4 0.0 copy-start.5
  196.4 0.0 copy-start.6
  196.4 0.0 copy-start.8
  196.4 0.0 copy-start.10
  196.5 78.2 %all-gather.8.cloned.1.call-done = bf16[384,2048]{0,1:T(8,128)(2,1)} async-done(((bf16[384,32]{0,1:T(8,128)(2,1)}), bf16[384,2048]{0,1:T(8,128)(2,1)}) %all-gather.8.cloned.1.call-update) | async-done | bytes 1572880 | tf_op jit(solution)/shard_map/all_gather | solution.py:129
  274.7 0.0 copy-done.5
  274.7 0.0 copy-done.8
  274.7 2.9 convolution_convert_fusion
  277.6 0.1 copy.41
  277.7 29.6 %all_to_all.38 = bf16[8,384,256]{2,1,0:T(8,128)(2,1)S(1)} all-to-all(bf16[8,384,256]{2,1,0:T(8,128)(2,1)S(1)} %bitcast.45), channel_id=1, replica_groups=mesh['fs'=64,'tp'=8] {'tp'}, dimensions={0} | all-to-all | bytes 3145728 | tf_op jit(solution)/shard_map/all_to_all | solution.py:55
  307.3 0.2 convert_reduce_fusion
  307.5 0.2 fusion.35
  307.7 0.6 broadcast_in_dim.73
  308.3 4.3 %all-to-all-start.6 = ((f32[8,1,768]{2,1,0:T(1,128)}), f32[8,1,768]{2,1,0:T(1,128)S(1)}, u32[]{:S(2)}, u32[]{:S(2)}) async-start(f32[8,1,768]{2,1,0:T(1,128)} %broadcast_in_dim.73), calls=%async_computation.6 | async-start | bytes 49152 | tf_op jit(solution)/shard_map/all_to_all | solution.py:13
  312.6 4.7 %all-to-all-done.6 = f32[8,1,768]{2,1,0:T(1,128)S(1)} async-done(((f32[8,1,768]{2,1,0:T(1,128)}), f32[8,1,768]{2,1,0:T(1,128)S(1)}, u32[]{:S(2)}, u32[]{:S(2)}) %all-to-all-start.6) | async-done | bytes 24608 | tf_op jit(solution)/shard_map/all_to_all | solution.py:13
  317.4 0.9 multiply_convert_fusion.1
  (27 shorter events, 0.3 us)
Async XLA Ops:
  6.5 101.5 %all-gather.4.cloned.1.call-start = ((), (), s32[]{:S(2)}) async-start(), calls=%async_computation.7 | async-start | bytes 3194880 | tf_op jit(solution)/shard_map/all_gather | solution.py:31
  7.9 184.7 %all-gather.6.cloned.1.call-start = ((), (), s32[]{:S(2)}) async-start(), calls=%async_computation.8 | async-start | bytes 3194880 | tf_op jit(solution)/shard_map/all_gather | solution.py:31
  10.6 29.8 %copy-start.1 = (bf16[256,32]{0,1:T(8,128)(2,1)S(1)}, bf16[256,32]{0,1:T(8,128)(2,1)}, u32[]{:S(2)}) copy-start(bf16[256,32]{0,1:T(8,128)(2,1)} %param.18) | copy-start | bytes 49156
  40.5 13.8 %copy-start.2 = (bf16[3,256]{1,0:T(4,128)(2,1)S(1)}, bf16[3,256]{1,0:T(4,128)(2,1)}, u32[]{:S(2)}) copy-start(bf16[3,256]{1,0:T(4,128)(2,1)} %param.17) | copy-start | bytes 4612
  41.6 72.4 %all-to-all-start.1 = ((bf16[64,256,32]{1,2,0:T(8,128)(2,1)}), bf16[64,256,32]{1,2,0:T(8,128)(2,1)S(1)}, u32[]{:S(2)}, u32[]{:S(2)}) async-start(bf16[64,256,32]{1,2,0:T(8,128)(2,1)} %broadcast_in_dim.68), calls=%async_computation.1 | async-start | bytes 2097152 | tf_op jit(solution)/shard_map/all_to_all | solution.py:13
  54.3 59.7 %copy-start.7 = (pred[384]{0:T(512)(128)(4,1)}, pred[384]{0:T(512)(128)(4,1)S(1)}, u32[]{:S(2)}) copy-start(pred[384]{0:T(512)(128)(4,1)S(1)} %get-tuple-element.22) | copy-start | bytes 1156
  54.3 59.7 %copy-start.9 = (pred[384]{0:T(512)(128)(4,1)}, pred[384]{0:T(512)(128)(4,1)S(1)}, u32[]{:S(2)}) copy-start(pred[384]{0:T(512)(128)(4,1)S(1)} %get-tuple-element.23) | copy-start | bytes 1156
  116.3 29.2 %all-to-all-start.2 = ((bf16[8,384,256]{2,1,0:T(8,128)(2,1)}), bf16[8,384,256]{2,1,0:T(8,128)(2,1)S(1)}, u32[]{:S(2)}, u32[]{:S(2)}) async-start(bf16[8,384,256]{2,1,0:T(8,128)(2,1)} %bitcast.38), calls=%async_computation.2 | async-start | bytes 3145728 | tf_op jit(solution)/shard_map/all_to_all | solution.py:55
  124.9 20.8 %copy-start = (bf16[384,256]{1,0:T(8,128)(2,1)S(1)}, bf16[384,256]{1,0:T(8,128)(2,1)}, u32[]{:S(2)}) copy-start(bf16[384,256]{1,0:T(8,128)(2,1)} %param.13) | copy-start | bytes 589828
  124.9 25.9 %copy-start.12 = (bf16[256]{0:T(256)(128)(2,1)S(1)}, bf16[256]{0:T(256)(128)(2,1)}, u32[]{:S(2)}) copy-start(bf16[256]{0:T(256)(128)(2,1)} %param.19) | copy-start | bytes 1540
  124.9 149.7 %all-gather.8.cloned.1.call-start = ((), (), s32[]{:S(2)}) async-start(), calls=%async_computation.9 | async-start | bytes 1597440 | tf_op jit(solution)/shard_map/all_gather | solution.py:129
  146.6 8.9 %all-to-all-start.3 = ((f32[8,1,768]{2,1,0:T(1,128)}), f32[8,1,768]{2,1,0:T(1,128)S(1)}, u32[]{:S(2)}, u32[]{:S(2)}) async-start(f32[8,1,768]{2,1,0:T(1,128)} %broadcast_in_dim.69), calls=%async_computation.3 | async-start | bytes 49152 | tf_op jit(solution)/shard_map/all_to_all | solution.py:13
  157.2 4.3 %copy-start.3 = (bf16[3,384]{1,0:T(4,128)(2,1)S(1)}, bf16[3,384]{1,0:T(4,128)(2,1)}, u32[]{:S(2)}) copy-start(bf16[3,384]{1,0:T(4,128)(2,1)} %param.22) | copy-start | bytes 6916
  157.2 4.3 %copy-start.4 = (bf16[3,384]{1,0:T(4,128)(2,1)S(1)}, bf16[3,384]{1,0:T(4,128)(2,1)}, u32[]{:S(2)}) copy-start(bf16[3,384]{1,0:T(4,128)(2,1)} %param.23) | copy-start | bytes 6916
  157.2 35.5 %all-to-all-start.4 = ((bf16[8,384,256]{1,2,0:T(8,128)(2,1)}), bf16[8,384,256]{1,2,0:T(8,128)(2,1)S(1)}, u32[]{:S(2)}, u32[]{:S(2)}) async-start(bf16[8,384,256]{1,2,0:T(8,128)(2,1)} %broadcast_in_dim.70), calls=%async_computation.4 | async-start | bytes 3145728 | tf_op jit(solution)/shard_map/all_to_all | solution.py:13
  192.7 2.7 copy-start.11
  196.4 78.3 %copy-start.5 = (f32[384]{0:T(512)S(1)}, f32[384]{0:T(512)}, u32[]{:S(2)}) copy-start(f32[384]{0:T(512)} %get-tuple-element.25) | copy-start | bytes 4612
  196.4 78.3 %copy-start.6 = (f32[384]{0:T(512)S(1)}, f32[384]{0:T(512)}, u32[]{:S(2)}) copy-start(f32[384]{0:T(512)} %get-tuple-element.26) | copy-start | bytes 4612
  196.4 78.3 %copy-start.8 = (pred[384]{0:T(512)(128)(4,1)S(1)}, pred[384]{0:T(512)(128)(4,1)}, u32[]{:S(2)}) copy-start(pred[384]{0:T(512)(128)(4,1)} %copy-done.7) | copy-start | bytes 1156
  196.4 78.3 %copy-start.10 = (pred[384]{0:T(512)(128)(4,1)S(1)}, pred[384]{0:T(512)(128)(4,1)}, u32[]{:S(2)}) copy-start(pred[384]{0:T(512)(128)(4,1)} %copy-done.9) | copy-start | bytes 1156
  307.3 5.3 %copy-start.13 = (bf16[256]{0:T(256)(128)(2,1)S(1)}, bf16[256]{0:T(256)(128)(2,1)}, u32[]{:S(2)}) copy-start(bf16[256]{0:T(256)(128)(2,1)} %param.25) | copy-start | bytes 1540
  308.3 9.0 %all-to-all-start.6 = ((f32[8,1,768]{2,1,0:T(1,128)}), f32[8,1,768]{2,1,0:T(1,128)S(1)}, u32[]{:S(2)}, u32[]{:S(2)}) async-start(f32[8,1,768]{2,1,0:T(1,128)} %broadcast_in_dim.73), calls=%async_computation.6 | async-start | bytes 49152 | tf_op jit(solution)/shard_map/all_to_all | solution.py:13
Sparse Core Ops, SparseCore 0:
  10.3 97.6 all-gather.3
  111.0 81.5 all-gather.5
  195.7 78.9 all-gather.7
where the time goes:
time: 326 us; the launch traced here: 325 us
  waiting for transfers between devices  192 us (59%)
  blocking collectives  59.4 us (18%)
  starting transfers between devices  34.1 us (10%)
  matrix products  13.4 us (4%)
  between operations  13.4 us (4%)
  local copies, waits for them, and re-layouts  7.32 us (2%)
  other arithmetic  4.73 us (1%)
    all_gather x2, waiting for transfers between devices, in_one_piece(): lax.all_gather(both, axis, axis=dim, tiled=True)  84.2 us
    all_gather x1, waiting for transfers between devices, body(): lax.all_gather(ffn_down, 'fs', axis=1, tiled=True)  78.2 us
    all_to_all x1, blocking collectives, copy_for_each(): return lax.all_to_all(copies, axis, split_axis=0, concat_axis=0, tiled=True)  29.8 us
    all_to_all x1, blocking collectives, sent_and_summed(): blocks = lax.all_to_all(split_up(value, dim, peers), axis, 0, 0, tiled=True)  29.6 us
    all_to_all x4, starting transfers between devices, copy_for_each(): return lax.all_to_all(copies, axis, split_axis=0, concat_axis=0, tiled=True)  25.5 us
    all_to_all x1, waiting for transfers between devices, sent_and_summed(): blocks = lax.all_to_all(split_up(value, dim, peers), axis, 0, 0, tiled=True)  19.8 us
    all_to_all x4, waiting for transfers between devices, copy_for_each(): return lax.all_to_all(copies, axis, split_axis=0, concat_axis=0, tiled=True)  9.4 us
    all_to_all x1, starting transfers between devices, sent_and_summed(): blocks = lax.all_to_all(split_up(value, dim, peers), axis, 0, 0, tiled=True)  8.57 us
  transfers between devices with their start and end apart: 8, of which 6 were waited for; matrix products, arithmetic and copies ran while one was open for 6% of the time, Pallas kernels for 0%

commit v1 on v0

--- a/solution.py
+++ b/solution.py
@@ -6,6 +6,27 @@
 SEQ_LEN = 128
 residual_scale = 8.0**0.25
 norm_epsilon = 1e-05
+
+
+def in_order(blocks, dim):
+    dims = list(blocks.shape[1:])
+    dims[dim] *= blocks.shape[0]
+    return jnp.moveaxis(blocks, 0, dim).reshape(dims)
+
+
+def collected_by_bits(x, axis):
+    devices, index = (lax.axis_size(axis), lax.axis_index(axis))
+    parts, apart = (x[None], 1)
+    while apart < devices:
+        other = lax.ppermute(parts, axis, [(i, i ^ apart) for i in range(devices)])
+        low = index & apart == 0
+        parts = jnp.concatenate([jnp.where(low, parts, other), jnp.where(low, other, parts)])
+        apart *= 2
+    return parts
+
+
+def gather_by_bits(x, axis, dim):
+    return in_order(collected_by_bits(x, axis), dim)
 
 
 def copy_for_each(value, axis):
@@ -125,9 +146,7 @@
         jax.nn.silu(causal_taps(gate_up, gate_taps)) * causal_taps(value_up, value_taps)
     ).astype(jnp.bfloat16)
     ffn_terms = jnp.dot(
-        hidden,
-        lax.all_gather(ffn_down, "fs", axis=1, tiled=True),
-        preferred_element_type=jnp.float32,
+        hidden, gather_by_bits(ffn_down, "fs", 1), preferred_element_type=jnp.float32
     )
     ffn_branch = sent_and_summed(ffn_terms.astype(jnp.bfloat16), "tp", 1)
     return norm_shares(residual_scale * first_own.astype(jnp.float32) + ffn_branch, ffn_gain)

time: 326 us -> 287 us (0.88)
  the two profiles are of different devices: /device:TPU:1 before, /device:TPU:56 now
where the time goes in v1:
time: 287 us; the launch traced here: 286 us
  waiting for transfers between devices  134 us (47%)
  starting transfers between devices  60.6 us (21%)
  blocking collectives  51.5 us (18%)
  matrix products  13.9 us (5%)
  between operations  13.9 us (5%)
  local copies, waits for them, and re-layouts  6.68 us (2%)
  other arithmetic  4.79 us (2%)
    ppermute x6, waiting for transfers between devices, collected_by_bits(): other = lax.ppermute(parts, axis, [(i, i ^ apart) for i in range(devices)])  92.1 us
    all_gather x2, waiting for transfers between devices, in_one_piece(): lax.all_gather(both, axis, axis=dim, tiled=True)  36.9 us
    all_to_all x4, starting transfers between devices, copy_for_each(): return lax.all_to_all(copies, axis, split_axis=0, concat_axis=0, tiled=True)  28.3 us
    ppermute x6, starting transfers between devices, collected_by_bits(): other = lax.ppermute(parts, axis, [(i, i ^ apart) for i in range(devices)])  27.9 us
    all_to_all x1, blocking collectives, sent_and_summed(): blocks = lax.all_to_all(split_up(value, dim, peers), axis, 0, 0, tiled=True)  25.8 us
    all_to_all x1, blocking collectives, copy_for_each(): return lax.all_to_all(copies, axis, split_axis=0, concat_axis=0, tiled=True)  25.7 us
    dot_general x3, matrix products, fold_rows(): jnp.dot(whole, piece, preferred_element_type=jnp.float32)  5.91 us
  transfers between devices with their start and end apart: 13, of which 8 were waited for; matrix products, arithmetic and copies ran while one was open for 5% of the time, Pallas kernels for 0%

profile of v1, /device:TPU:56, one launch (start us, length us, event | category | flops | bytes accessed | tf_op | source)
XLA Modules:
  0.0 285.9 jit_solution(9932793783260116492)
XLA Ops:
  6.5 0.0 all-gather.3.cloned.1.call-start
  6.5 1.4 pad_maximum_fusion.5
  7.9 0.0 all-gather.3.cloned.1.call-update
  7.9 1.1 copy.25
  9.0 0.1 broadcast_in_dim.68
  9.2 0.0 copy-start.4
  9.2 25.7 %all_to_all.37 = bf16[8,384,256]{1,2,0:T(8,128)(2,1)S(1)} all-to-all(bf16[8,384,256]{1,2,0:T(8,128)(2,1)S(1)} %broadcast_in_dim.68), channel_id=1, replica_groups=mesh['fs'=64,'tp'=8] {'tp'}, dimensions={0} | all-to-all | bytes 3145728 | tf_op jit(solution)/shard_map/all_to_all | solution.py:34
  34.9 0.0 copy-start.5
  34.9 1.1 broadcast_in_dim.71
  36.0 15.9 %all-to-all-start.1 = ((bf16[64,256,32]{1,2,0:T(8,128)(2,1)}), bf16[64,256,32]{1,2,0:T(8,128)(2,1)S(1)}, u32[]{:S(2)}, u32[]{:S(2)}) async-start(bf16[64,256,32]{1,2,0:T(8,128)(2,1)} %broadcast_in_dim.71), calls=%async_computation.1 | async-start | bytes 2097152 | tf_op jit(solution)/shard_map/all_to_all | solution.py:34
  51.9 0.0 all-gather.5.cloned.1.call-start
  52.0 0.6 pad_maximum_fusion.6
  52.6 0.1 all-gather.5.cloned.1.call-update
  52.7 3.4 %collective-permute-start = (bf16[1,384,32]{1,2,0:T(8,128)(2,1)S(1)}, bf16[1,384,32]{1,2,0:T(8,128)(2,1)S(1)}, u32[]{:S(2)}, u32[]{:S(2)}) collective-permute-start(bf16[1,384,32]{1,2,0:T(8,128)(2,1)S(1)} %bitcast.57), channel_id=1, source_target_pairs={{0,8},{8,0},{16,24},{24,16},{32,40},{40,32},{48,56},{56,48},{64,72... | collective-permute-start | bytes 73736 | tf_op jit(solution)/shard_map/ppermute | solution.py:21
  56.1 19.5 %collective-permute-done = bf16[1,384,32]{1,2,0:T(8,128)(2,1)S(1)} collective-permute-done((bf16[1,384,32]{1,2,0:T(8,128)(2,1)S(1)}, bf16[1,384,32]{1,2,0:T(8,128)(2,1)S(1)}, u32[]{:S(2)}, u32[]{:S(2)}) %collective-permute-start) | collective-permute-done | bytes 24608 | tf_op jit(solution)/shard_map/ppermute | solution.py:21
  75.7 36.9 %all-gather.3.cloned.1.call-done = bf16[2048,768]{1,0:T(8,128)(2,1)} async-done(((bf16[32,768]{1,0:T(8,128)(2,1)}), bf16[2048,768]{1,0:T(8,128)(2,1)}) %all-gather.3.cloned.1.call-update) | async-done | bytes 3145744 | tf_op jit(solution)/shard_map/all_gather | solution.py:52
  112.6 2.0 fusion.11
  114.5 2.0 fusion.12
  116.5 2.0 fusion.10
  118.6 0.0 all-to-all-done.1
  118.6 1.1 convolution_convert_fusion.1
  119.6 1.2 copy.42
  120.9 4.4 %all-to-all-start.2 = ((bf16[8,384,256]{2,1,0:T(8,128)(2,1)}), bf16[8,384,256]{2,1,0:T(8,128)(2,1)S(1)}, u32[]{:S(2)}, u32[]{:S(2)}) async-start(bf16[8,384,256]{2,1,0:T(8,128)(2,1)} %bitcast.44), calls=%async_computation.2 | async-start | bytes 3145728 | tf_op jit(solution)/shard_map/all_to_all | solution.py:76
  125.3 3.7 %collective-permute-start.1 = (bf16[2,384,32]{1,2,0:T(8,128)(2,1)S(1)}, bf16[2,384,32]{1,2,0:T(8,128)(2,1)S(1)}, u32[]{:S(2)}, u32[]{:S(2)}) collective-permute-start(bf16[2,384,32]{1,2,0:T(8,128)(2,1)S(1)} %pad_maximum_fusion.7), channel_id=1, source_target_pairs={{0,16},{8,24},{16,0},{24,8},{32,48},{40,56},{48,32},{56,40},{64,80... | collective-permute-start | bytes 147464 | tf_op jit(solution)/shard_map/ppermute | solution.py:21
  129.0 4.6 %collective-permute-done.1 = bf16[2,384,32]{1,2,0:T(8,128)(2,1)S(1)} collective-permute-done((bf16[2,384,32]{1,2,0:T(8,128)(2,1)S(1)}, bf16[2,384,32]{1,2,0:T(8,128)(2,1)S(1)}, u32[]{:S(2)}, u32[]{:S(2)}) %collective-permute-start.1) | collective-permute-done | bytes 49184 | tf_op jit(solution)/shard_map/ppermute | solution.py:21
  133.6 5.5 %collective-permute-start.2 = (bf16[4,384,32]{1,2,0:T(8,128)(2,1)S(1)}, bf16[4,384,32]{1,2,0:T(8,128)(2,1)S(1)}, u32[]{:S(2)}, u32[]{:S(2)}) collective-permute-start(bf16[4,384,32]{1,2,0:T(8,128)(2,1)S(1)} %pad_maximum_fusion.4), channel_id=1, source_target_pairs={{0,32},{8,40},{16,48},{24,56},{32,0},{40,8},{48,16},{56,24},{64,96... | collective-permute-start | bytes 294920 | tf_op jit(solution)/shard_map/ppermute | solution.py:21
  139.1 6.3 %collective-permute-done.2 = bf16[4,384,32]{1,2,0:T(8,128)(2,1)S(1)} collective-permute-done((bf16[4,384,32]{1,2,0:T(8,128)(2,1)S(1)}, bf16[4,384,32]{1,2,0:T(8,128)(2,1)S(1)}, u32[]{:S(2)}, u32[]{:S(2)}) %collective-permute-start.2) | collective-permute-done | bytes 98336 | tf_op jit(solution)/shard_map/ppermute | solution.py:21
  145.5 0.0 copy-start
  145.5 2.8 collective-permute-start.3
  148.3 5.0 %collective-permute-done.3 = bf16[8,384,32]{1,2,0:T(8,128)(2,1)S(1)} collective-permute-done((bf16[8,384,32]{1,2,0:T(8,128)(2,1)S(1)}, bf16[8,384,32]{1,2,0:T(8,128)(2,1)S(1)}, u32[]{:S(2)}, u32[]{:S(2)}) %collective-permute-start.3) | collective-permute-done | bytes 196640 | tf_op jit(solution)/shard_map/ppermute | solution.py:21
  153.4 0.1 broadcast_select_fusion.5
  153.4 0.0 all-to-all-done.2
  153.4 0.2 convert_reduce_fusion.1
  153.7 0.0 copy-done
  153.7 0.2 fusion.34
  153.9 0.6 broadcast_in_dim.72
  154.5 4.2 %all-to-all-start.3 = ((f32[8,1,768]{2,1,0:T(1,128)}), f32[8,1,768]{2,1,0:T(1,128)S(1)}, u32[]{:S(2)}, u32[]{:S(2)}) async-start(f32[8,1,768]{2,1,0:T(1,128)} %broadcast_in_dim.72), calls=%async_computation.3 | async-start | bytes 49152 | tf_op jit(solution)/shard_map/all_to_all | solution.py:34
  158.8 5.6 %collective-permute-start.4 = (bf16[16,384,32]{1,2,0:T(8,128)(2,1)S(1)}, bf16[16,384,32]{1,2,0:T(8,128)(2,1)S(1)}, u32[]{:S(2)}, u32[]{:S(2)}) collective-permute-start(bf16[16,384,32]{1,2,0:T(8,128)(2,1)S(1)} %pad_maximum_fusion.2), channel_id=1, source_target_pairs={{0,128},{8,136},{16,144},{24,152},{32,160},{40,168},{48,176},{56,1... | collective-permute-start | bytes 1179656 | tf_op jit(solution)/shard_map/ppermute | solution.py:21
  164.4 0.0 all-to-all-done.3
  164.4 0.2 multiply_convert_fusion.2
  164.6 0.2 copy.28
  164.8 1.3 broadcast_in_dim.73
  166.1 4.8 %all-to-all-start.4 = ((bf16[8,384,256]{1,2,0:T(8,128)(2,1)}), bf16[8,384,256]{1,2,0:T(8,128)(2,1)}, u32[]{:S(2)}, u32[]{:S(2)}) async-start(bf16[8,384,256]{1,2,0:T(8,128)(2,1)} %broadcast_in_dim.73), calls=%async_computation.4 | async-start | bytes 3145728 | tf_op jit(solution)/shard_map/all_to_all | solution.py:34
  170.9 0.0 copy-start.7
  170.9 18.6 %collective-permute-done.4 = bf16[16,384,32]{1,2,0:T(8,128)(2,1)S(1)} collective-permute-done((bf16[16,384,32]{1,2,0:T(8,128)(2,1)S(1)}, bf16[16,384,32]{1,2,0:T(8,128)(2,1)S(1)}, u32[]{:S(2)}, u32[]{:S(2)}) %collective-permute-start.4) | collective-permute-done | bytes 393248 | tf_op jit(solution)/shard_map/ppermute | solution.py:21
  189.5 0.1 broadcast_select_fusion.3
  189.7 0.1 pad_maximum_fusion.1
  189.8 7.0 %collective-permute-start.5 = (bf16[32,384,32]{1,2,0:T(8,128)(2,1)S(1)}, bf16[32,384,32]{1,2,0:T(8,128)(2,1)S(1)}, u32[]{:S(2)}, u32[]{:S(2)}) collective-permute-start(bf16[32,384,32]{1,2,0:T(8,128)(2,1)S(1)} %pad_maximum_fusion.1), channel_id=1, source_target_pairs={{0,256},{8,264},{16,272},{24,280},{32,288},{40,296},{48,304},{56,3... | collective-permute-start | bytes 2359304 | tf_op jit(solution)/shard_map/ppermute | solution.py:21
  196.8 38.1 %collective-permute-done.5 = bf16[32,384,32]{1,2,0:T(8,128)(2,1)S(1)} collective-permute-done((bf16[32,384,32]{1,2,0:T(8,128)(2,1)S(1)}, bf16[32,384,32]{1,2,0:T(8,128)(2,1)S(1)}, u32[]{:S(2)}, u32[]{:S(2)}) %collective-permute-start.5) | collective-permute-done | bytes 786464 | tf_op jit(solution)/shard_map/ppermute | solution.py:21
  234.9 0.2 broadcast_select_fusion.1
  235.1 0.2 pad_maximum_fusion
  235.3 0.0 all-gather.5.cloned.1.call-done
  235.3 0.0 all-to-all-done.4
  235.3 3.0 %fusion.4 = bf16[384,384]{1,0:T(8,128)(2,1)S(1)} fusion(bf16[384,2048]{0,1:T(8,128)(2,1)} %bitcast.13, bf16[2048,768]{1,0:T(8,128)(2,1)} %all-gather.5.cloned.1.call-done), kind=kOutput, calls=%fused_computation.11 | convolution fusion | flops 604127232 | bytes 3440640 | tf_op jit(solution)/shard_map/dot_general | solution.py:142
  238.5 2.4 fusion.7
  241.0 1.5 convolution_convert_fusion
  242.5 0.1 copy.41
  242.6 25.8 %all_to_all.38 = bf16[8,384,256]{2,1,0:T(8,128)(2,1)S(1)} all-to-all(bf16[8,384,256]{2,1,0:T(8,128)(2,1)S(1)} %bitcast.51), channel_id=1, replica_groups=mesh['fs'=64,'tp'=8] {'tp'}, dimensions={0} | all-to-all | bytes 3145728 | tf_op jit(solution)/shard_map/all_to_all | solution.py:76
  268.4 0.2 convert_reduce_fusion
  268.7 0.2 fusion.35
  268.9 0.6 broadcast_in_dim.77
  269.5 3.3 %all-to-all-start.6 = ((f32[8,1,768]{2,1,0:T(1,128)}), f32[8,1,768]{2,1,0:T(1,128)S(1)}, u32[]{:S(2)}, u32[]{:S(2)}) async-start(f32[8,1,768]{2,1,0:T(1,128)} %broadcast_in_dim.77), calls=%async_computation.6 | async-start | bytes 49152 | tf_op jit(solution)/shard_map/all_to_all | solution.py:34
  272.9 5.3 %all-to-all-done.6 = f32[8,1,768]{2,1,0:T(1,128)S(1)} async-done(((f32[8,1,768]{2,1,0:T(1,128)}), f32[8,1,768]{2,1,0:T(1,128)S(1)}, u32[]{:S(2)}, u32[]{:S(2)}) %all-to-all-start.6) | async-done | bytes 24608 | tf_op jit(solution)/shard_map/all_to_all | solution.py:34
  278.2 0.9 multiply_convert_fusion.1
  (42 shorter events, 0.6 us)
Async XLA Ops:
  6.5 106.0 %all-gather.3.cloned.1.call-start = ((), (), s32[]{:S(2)}) async-start(), calls=%async_computation.7 | async-start | bytes 3194880 | tf_op jit(solution)/shard_map/all_gather | solution.py:52
  9.2 25.7 %copy-start.4 = (bf16[256,32]{0,1:T(8,128)(2,1)S(1)}, bf16[256,32]{0,1:T(8,128)(2,1)}, u32[]{:S(2)}) copy-start(bf16[256,32]{0,1:T(8,128)(2,1)} %param.18) | copy-start | bytes 49156
  34.9 17.1 %copy-start.1 = (bf16[32,384]{1,0:T(8,128)(2,1)S(1)}, bf16[32,384]{1,0:T(8,128)(2,1)}, u32[]{:S(2)}) copy-start(bf16[32,384]{1,0:T(8,128)(2,1)} %param.21) | copy-start | bytes 73732
  34.9 17.1 %copy-start.2 = (bf16[32,384]{1,0:T(8,128)(2,1)S(1)}, bf16[32,384]{1,0:T(8,128)(2,1)}, u32[]{:S(2)}) copy-start(bf16[32,384]{1,0:T(8,128)(2,1)} %param.20) | copy-start | bytes 73732
  34.9 17.8 %copy-start.3 = (bf16[384,32]{0,1:T(8,128)(2,1)S(1)}, bf16[384,32]{0,1:T(8,128)(2,1)}, u32[]{:S(2)}) copy-start(bf16[384,32]{0,1:T(8,128)(2,1)} %param.24) | copy-start | bytes 73732
  34.9 21.2 %copy-start.5 = (bf16[3,256]{1,0:T(4,128)(2,1)S(1)}, bf16[3,256]{1,0:T(4,128)(2,1)}, u32[]{:S(2)}) copy-start(bf16[3,256]{1,0:T(4,128)(2,1)} %param.17) | copy-start | bytes 4612
  36.0 82.5 %all-to-all-start.1 = ((bf16[64,256,32]{1,2,0:T(8,128)(2,1)}), bf16[64,256,32]{1,2,0:T(8,128)(2,1)S(1)}, u32[]{:S(2)}, u32[]{:S(2)}) async-start(bf16[64,256,32]{1,2,0:T(8,128)(2,1)} %broadcast_in_dim.71), calls=%async_computation.1 | async-start | bytes 2097152 | tf_op jit(solution)/shard_map/all_to_all | solution.py:34
  51.9 183.4 %all-gather.5.cloned.1.call-start = ((), (), s32[]{:S(2)}) async-start(), calls=%async_computation.8 | async-start | bytes 3194880 | tf_op jit(solution)/shard_map/all_gather | solution.py:52
  52.7 23.0 %collective-permute-start = (bf16[1,384,32]{1,2,0:T(8,128)(2,1)S(1)}, bf16[1,384,32]{1,2,0:T(8,128)(2,1)S(1)}, u32[]{:S(2)}, u32[]{:S(2)}) collective-permute-start(bf16[1,384,32]{1,2,0:T(8,128)(2,1)S(1)} %bitcast.57), channel_id=1, source_target_pairs={{0,8},{8,0},{16,24},{24,16},{32,40},{40,32},{48,56},{56,48},{64,72... | collective-permute-start | bytes 73736 | tf_op jit(solution)/shard_map/ppermute | solution.py:21
  120.9 27.4 %copy-start.9 = (bf16[256]{0:T(256)(128)(2,1)S(1)}, bf16[256]{0:T(256)(128)(2,1)}, u32[]{:S(2)}) copy-start(bf16[256]{0:T(256)(128)(2,1)} %param.19) | copy-start | bytes 1540
  120.9 32.6 %all-to-all-start.2 = ((bf16[8,384,256]{2,1,0:T(8,128)(2,1)}), bf16[8,384,256]{2,1,0:T(8,128)(2,1)S(1)}, u32[]{:S(2)}, u32[]{:S(2)}) async-start(bf16[8,384,256]{2,1,0:T(8,128)(2,1)} %bitcast.44), calls=%async_computation.2 | async-start | bytes 3145728 | tf_op jit(solution)/shard_map/all_to_all | solution.py:76
  125.3 8.3 %collective-permute-start.1 = (bf16[2,384,32]{1,2,0:T(8,128)(2,1)S(1)}, bf16[2,384,32]{1,2,0:T(8,128)(2,1)S(1)}, u32[]{:S(2)}, u32[]{:S(2)}) collective-permute-start(bf16[2,384,32]{1,2,0:T(8,128)(2,1)S(1)} %pad_maximum_fusion.7), channel_id=1, source_target_pairs={{0,16},{8,24},{16,0},{24,8},{32,48},{40,56},{48,32},{56,40},{64,80... | collective-permute-start | bytes 147464 | tf_op jit(solution)/shard_map/ppermute | solution.py:21
  133.6 11.9 %collective-permute-start.2 = (bf16[4,384,32]{1,2,0:T(8,128)(2,1)S(1)}, bf16[4,384,32]{1,2,0:T(8,128)(2,1)S(1)}, u32[]{:S(2)}, u32[]{:S(2)}) collective-permute-start(bf16[4,384,32]{1,2,0:T(8,128)(2,1)S(1)} %pad_maximum_fusion.4), channel_id=1, source_target_pairs={{0,32},{8,40},{16,48},{24,56},{32,0},{40,8},{48,16},{56,24},{64,96... | collective-permute-start | bytes 294920 | tf_op jit(solution)/shard_map/ppermute | solution.py:21
  145.5 8.2 %copy-start = (bf16[384,256]{1,0:T(8,128)(2,1)S(1)}, bf16[384,256]{1,0:T(8,128)(2,1)}, u32[]{:S(2)}) copy-start(bf16[384,256]{1,0:T(8,128)(2,1)} %param.13) | copy-start | bytes 589828
  145.5 7.9 %collective-permute-start.3 = (bf16[8,384,32]{1,2,0:T(8,128)(2,1)S(1)}, bf16[8,384,32]{1,2,0:T(8,128)(2,1)S(1)}, u32[]{:S(2)}, u32[]{:S(2)}) collective-permute-start(bf16[8,384,32]{1,2,0:T(8,128)(2,1)S(1)} %pad_maximum_fusion.3), channel_id=1, source_target_pairs={{0,64},{8,72},{16,80},{24,88},{32,96},{40,104},{48,112},{56,120},{... | collective-permute-start | bytes 589832 | tf_op jit(solution)/shard_map/ppermute | solution.py:21
  154.5 9.9 %all-to-all-start.3 = ((f32[8,1,768]{2,1,0:T(1,128)}), f32[8,1,768]{2,1,0:T(1,128)S(1)}, u32[]{:S(2)}, u32[]{:S(2)}) async-start(f32[8,1,768]{2,1,0:T(1,128)} %broadcast_in_dim.72), calls=%async_computation.3 | async-start | bytes 49152 | tf_op jit(solution)/shard_map/all_to_all | solution.py:34
  158.8 30.7 %collective-permute-start.4 = (bf16[16,384,32]{1,2,0:T(8,128)(2,1)S(1)}, bf16[16,384,32]{1,2,0:T(8,128)(2,1)S(1)}, u32[]{:S(2)}, u32[]{:S(2)}) collective-permute-start(bf16[16,384,32]{1,2,0:T(8,128)(2,1)S(1)} %pad_maximum_fusion.2), channel_id=1, source_target_pairs={{0,128},{8,136},{16,144},{24,152},{32,160},{40,168},{48,176},{56,1... | collective-permute-start | bytes 1179656 | tf_op jit(solution)/shard_map/ppermute | solution.py:21
  166.1 69.2 %all-to-all-start.4 = ((bf16[8,384,256]{1,2,0:T(8,128)(2,1)}), bf16[8,384,256]{1,2,0:T(8,128)(2,1)}, u32[]{:S(2)}, u32[]{:S(2)}) async-start(bf16[8,384,256]{1,2,0:T(8,128)(2,1)} %broadcast_in_dim.73), calls=%async_computation.4 | async-start | bytes 3145728 | tf_op jit(solution)/shard_map/all_to_all | solution.py:34
  170.9 25.8 %copy-start.6 = (bf16[3,384]{1,0:T(4,128)(2,1)S(1)}, bf16[3,384]{1,0:T(4,128)(2,1)}, u32[]{:S(2)}) copy-start(bf16[3,384]{1,0:T(4,128)(2,1)} %param.22) | copy-start | bytes 6916
  170.9 25.9 %copy-start.7 = (bf16[3,384]{1,0:T(4,128)(2,1)S(1)}, bf16[3,384]{1,0:T(4,128)(2,1)}, u32[]{:S(2)}) copy-start(bf16[3,384]{1,0:T(4,128)(2,1)} %param.23) | copy-start | bytes 6916
  189.8 45.1 %collective-permute-start.5 = (bf16[32,384,32]{1,2,0:T(8,128)(2,1)S(1)}, bf16[32,384,32]{1,2,0:T(8,128)(2,1)S(1)}, u32[]{:S(2)}, u32[]{:S(2)}) collective-permute-start(bf16[32,384,32]{1,2,0:T(8,128)(2,1)S(1)} %pad_maximum_fusion.1), channel_id=1, source_target_pairs={{0,256},{8,264},{16,272},{24,280},{32,288},{40,296},{48,304},{56,3... | collective-permute-start | bytes 2359304 | tf_op jit(solution)/shard_map/ppermute | solution.py:21
  235.3 3.1 %copy-start.8 = (bf16[2048,768]{1,0:T(8,128)(2,1)S(1)}, bf16[2048,768]{1,0:T(8,128)(2,1)}, u32[]{:S(2)}) copy-start(bf16[2048,768]{1,0:T(8,128)(2,1)} %all-gather.5.cloned.1.call-done) | copy-start | bytes 9437188
  268.4 4.4 %copy-start.10 = (bf16[256]{0:T(256)(128)(2,1)S(1)}, bf16[256]{0:T(256)(128)(2,1)}, u32[]{:S(2)}) copy-start(bf16[256]{0:T(256)(128)(2,1)} %param.25) | copy-start | bytes 1540
  269.5 8.7 %all-to-all-start.6 = ((f32[8,1,768]{2,1,0:T(1,128)}), f32[8,1,768]{2,1,0:T(1,128)S(1)}, u32[]{:S(2)}, u32[]{:S(2)}) async-start(f32[8,1,768]{2,1,0:T(1,128)} %broadcast_in_dim.77), calls=%async_computation.6 | async-start | bytes 49152 | tf_op jit(solution)/shard_map/all_to_all | solution.py:34
Sparse Core Ops, SparseCore 0:
  10.3 102.1 all-gather.2
  115.6 110.0 all-gather.4
